TPU v7x, 32 devices: a whole 2x2x4 slice. The times are simulated.
32 devices in a mesh: row: 8 (over z, x), col: 4 (over y, core).
Axes of the slice: x: 2, y: 2, z: 4, core: 2. Of those that a mesh axis runs over, the one named last changes fastest.
Arguments:
- tokens: bfloat16 [8192, 2048], P('row'), may hold values from -136 to 136
- norm_gain: float32 [2048], replicated, may hold values from 0.1 to 1.9
- w_in: bfloat16 [2048, 1024], P(None, 'col'), may hold values from -0.125 to 0.125
- w_out: bfloat16 [1024, 2048], P(None, 'col'), may hold values from -0.1875 to 0.1875
Outputs:
- mixed_tokens: bfloat16 [8192, 2048], P('row', 'col')
All inputs are finite; a program needn't handle non-finite values.
Results may differ from a plain program's by a relative error of at most 0.013.
Values may be sent and summed in bfloat16 or wider, within the bound.
A program may use at most 64 MiB of HBM per device.

v0:
```python
import math

import jax
import jax.numpy as jnp
from jax import lax
from jax.sharding import PartitionSpec as P

GROUP = 256


NORM_EPS = 1e-06


def as_sent(array):

    def short(part):
        return part.astype(jnp.bfloat16) if part.dtype == jnp.float32 else part

    return jax.tree.map(short, array)


def rotation_table(first_index, second_index, spectral_magnitude, factor):
    phase = (first_index * second_index % spectral_magnitude).astype(jnp.float32) * (
        2.0 * math.pi / spectral_magnitude
    )
    return (jnp.cos(phase) * factor, jnp.sin(phase) * factor)


def twiddle(real_input_values, imag_in, freq_index, pos_index, spectral_magnitude):
    cosine, sine = rotation_table(freq_index, pos_index, spectral_magnitude, 1.0)
    return (
        real_input_values * cosine + imag_in * sine,
        imag_in * cosine - real_input_values * sine,
    )


def second_section(stacked, half):
    length_dev = stacked.shape[1]
    stride = min(length_dev, 512)
    positions = lax.broadcasted_iota(jnp.int32, (length_dev, stride), 0)
    real_blocks = []
    imag_blocks = []
    for offset in range(0, length_dev, stride):
        freqs = lax.broadcasted_iota(jnp.int32, (length_dev, stride), 1) + offset
        cosine, sine = rotation_table(positions, freqs, length_dev, 1.0)
        with_cos = jnp.dot(stacked, cosine, precision=lax.Precision.HIGH)
        with_sin = jnp.dot(stacked, sine, precision=lax.Precision.HIGH)
        real_blocks.append(with_cos[:half] + with_sin[half:])
        imag_blocks.append(with_cos[half:] - with_sin[:half])
    return (jnp.concatenate(real_blocks, 1), jnp.concatenate(imag_blocks, 1))


def reorder_positions(arrived):
    channels, row_count, _, block_len = arrived.shape
    return jnp.swapaxes(arrived.reshape(channels, row_count, block_len), 1, 2).reshape(
        channels, row_count * block_len
    )


def local(tokens, norm_gain, w_in, w_out):
    length_dev = tokens.shape[0]
    row_count = lax.axis_size("row")
    col_count = lax.axis_size("col")
    total_len = length_dev * row_count
    widened = tokens.astype(jnp.float32)
    inverse = lax.rsqrt(jnp.mean(widened * widened, axis=1, keepdims=True) + NORM_EPS)
    normed = (widened * inverse * norm_gain[None, :]).astype(jnp.bfloat16)
    projected = lax.dot_general(
        w_in, normed, (((0,), (1,)), ((), ())), preferred_element_type=jnp.float32
    ).astype(jnp.bfloat16)
    channels = projected.shape[0]
    block_len = length_dev // row_count
    small_cos, small_sin = rotation_table(
        lax.broadcasted_iota(jnp.int32, (row_count, row_count), 0),
        lax.broadcasted_iota(jnp.int32, (row_count, row_count), 1),
        row_count,
        1.0 / math.sqrt(total_len),
    )
    per_row = channels // row_count
    arrived = lax.all_to_all(
        projected.reshape(channels, 1, length_dev), "row", split_axis=0, concat_axis=1, tiled=True
    )
    values = arrived.astype(jnp.float32)
    real_one = jnp.einsum("ka,cab->ckb", small_cos, values, precision=lax.Precision.HIGH)
    imag_one = -jnp.einsum("ka,cab->ckb", small_sin, values, precision=lax.Precision.HIGH)
    freq_index = lax.broadcasted_iota(jnp.int32, (row_count, length_dev), 0)
    pos_index = lax.broadcasted_iota(jnp.int32, (row_count, length_dev), 1)
    real_two, imag_two = twiddle(real_one, imag_one, freq_index, pos_index, total_len)
    stacked = jnp.concatenate(
        [
            real_two.reshape(per_row * row_count, length_dev),
            imag_two.reshape(per_row * row_count, length_dev),
        ],
        0,
    )
    real_three, imag_three = second_section(stacked, per_row * row_count)
    shaped = (per_row, row_count, row_count, block_len)
    back_real, back_imag = (
        lax.all_to_all(
            real_three.reshape(shaped).astype(jnp.bfloat16),
            "row",
            split_axis=2,
            concat_axis=0,
            tiled=True,
        ).astype(jnp.float32),
        lax.all_to_all(
            imag_three.reshape(shaped).astype(jnp.bfloat16),
            "row",
            split_axis=2,
            concat_axis=0,
            tiled=True,
        ).astype(jnp.float32),
    )
    spec_real = reorder_positions(back_real)
    spec_imag = reorder_positions(back_imag)
    quarter = length_dev // col_count
    group_cosine_table, group_sine_table = rotation_table(
        lax.broadcasted_iota(jnp.int32, (GROUP, GROUP), 0),
        lax.broadcasted_iota(jnp.int32, (GROUP, GROUP), 1),
        GROUP,
        1.0 / math.sqrt(GROUP),
    )
    real_input_values = lax.all_to_all(
        as_sent(spec_real.reshape(channels, col_count, quarter)),
        "col",
        split_axis=1,
        concat_axis=0,
        tiled=True,
    )
    imag_in = lax.all_to_all(
        as_sent(spec_imag.reshape(channels, col_count, quarter)),
        "col",
        split_axis=1,
        concat_axis=0,
        tiled=True,
    )
    width_all = real_input_values.shape[0]
    item_count = real_input_values.shape[2]
    groups = width_all // GROUP
    real_by_group = real_input_values.reshape(groups, GROUP, item_count)
    imaginary_by_group = imag_in.reshape(groups, GROUP, item_count)
    merged_spectrum = jnp.einsum(
        "hz,azo->aho", group_cosine_table, real_by_group, precision=lax.Precision.HIGH
    )
    merged_spectrum = merged_spectrum + jnp.einsum(
        "hz,azo->aho", group_sine_table, imaginary_by_group, precision=lax.Precision.HIGH
    )
    result = merged_spectrum.reshape(width_all, 1, item_count).astype(jnp.bfloat16)
    spectral = lax.all_to_all(result, "col", split_axis=0, concat_axis=1, tiled=True)
    output = lax.dot_general(
        lax.all_gather(spectral.reshape(channels, length_dev), "col", axis=0, tiled=True),
        w_out,
        (((0,), (0,)), ((), ())),
        preferred_element_type=jnp.float32,
    )
    return output.astype(jnp.bfloat16)


def solution(mesh):
    placed = (P("row", None), P(), P(None, "col"), P(None, "col"))
    return jax.shard_map(
        local, mesh=mesh, in_specs=placed, out_specs=P("row", "col"), check_vma=False
    )
```

profile of v0, /device:TPU:0, one launch (start us, length us, event | category | flops | bytes accessed | tf_op | source)
XLA Modules:
  0.0 188.0 jit_solution(15366672297851264644)
XLA Ops:
  6.5 3.2 %fusion = f32[1024]{0:T(1024)S(1)} fusion(bf16[1024,2048]{1,0:T(8,128)(2,1)} %param.4), kind=kLoop, calls=%fused_computation.2 | loop fusion | flops 6290432 | bytes 4198400 | tf_op jit(solution)/shard_map/reduce_sum | solution.py:66
  10.1 2.5 %fusion.32 = bf16[256,1,1024]{0,2,1:T(8,128)(2,1)S(1)} fusion(bf16[2048,256]{1,0:T(8,128)(2,1)} %param.6, bf16[1024,2048]{1,0:T(8,128)(2,1)S(1)} %copy-done.1, f32[2048]{0:T(1024)S(1)} %copy-done.2, f32[1024]{0:T(1024)S(1)} %add_rsqrt_fusion), kind=kOutput, calls=%fused_computation.42 | convolution fusion | flops 1082392576 | bytes 5779456 | tf_op jit(solution)/shard_map/dot_general | solution.py:68
  13.2 1.0 reduce
  14.4 1.2 reshape.104
  15.6 7.3 %all-to-all-start = ((bf16[8,2,16384]{2,1,0:T(2,128)(2,1)}), bf16[8,2,16384]{2,1,0:T(2,128)(2,1)S(1)}, u32[]{:S(2)}, u32[]{:S(2)}) async-start(bf16[8,2,16384]{2,1,0:T(2,128)(2,1)} %reshape.104), calls=%async_computation | async-start | bytes 1048576 | tf_op jit(solution)/shard_map/all_to_all | solution.py:80
  23.0 14.3 %all-to-all-done = bf16[8,2,16384]{2,1,0:T(2,128)(2,1)S(1)} async-done(((bf16[8,2,16384]{2,1,0:T(2,128)(2,1)}), bf16[8,2,16384]{2,1,0:T(2,128)(2,1)S(1)}, u32[]{:S(2)}, u32[]{:S(2)}) %all-to-all-start) | async-done | bytes 524320 | tf_op jit(solution)/shard_map/all_to_all | solution.py:80
  40.0 9.2 %fusion.15 = f32[512,512]{0,1:T(8,128)S(1)} fusion(s32[512]{0:T(512)S(1)} %iota_add_fusion, f32[256,1024]{1,0:T(8,128)S(1)} %get-tuple-element.6, f32[256,1024]{1,0:T(8,128)S(1)} %get-tuple-element.5), kind=kOutput, calls=%fused_computation.23 | convolution fusion | flops 1618477056 | bytes 3147776 | tf_op jit(solution)/shard_map/dot_general | solution.py:46
  49.3 9.5 %fusion.13 = f32[512,512]{0,1:T(8,128)S(1)} fusion(s32[512]{0:T(512)S(1)} %iota_add_fusion, f32[256,1024]{1,0:T(8,128)S(1)} %get-tuple-element.6, f32[256,1024]{1,0:T(8,128)S(1)} %get-tuple-element.5), kind=kOutput, calls=%fused_computation.21 | convolution fusion | flops 1618477056 | bytes 3147776 | tf_op jit(solution)/shard_map/dot_general | solution.py:47
  58.7 9.7 %fusion.21 = f32[512,512]{0,1:T(8,128)S(1)} fusion(f32[256,1024]{1,0:T(8,128)S(1)} %get-tuple-element.6, f32[256,1024]{1,0:T(8,128)S(1)} %get-tuple-element.5), kind=kOutput, calls=%fused_computation.29 | convolution fusion | flops 1618477056 | bytes 3145728 | tf_op jit(solution)/shard_map/dot_general | solution.py:46
  68.4 9.5 %fusion.19 = f32[512,512]{0,1:T(8,128)S(1)} fusion(f32[256,1024]{1,0:T(8,128)S(1)} %get-tuple-element.6, f32[256,1024]{1,0:T(8,128)S(1)} %get-tuple-element.5), kind=kOutput, calls=%fused_computation.27 | convolution fusion | flops 1618477056 | bytes 3145728 | tf_op jit(solution)/shard_map/dot_general | solution.py:47
  79.5 3.6 %all-to-all-start.1 = ((bf16[32,8,8,128]{3,1,0,2:T(8,128)(2,1)}), bf16[32,8,8,128]{3,1,0,2:T(8,128)(2,1)S(1)}, u32[]{:S(2)}, u32[]{:S(2)}) async-start(bf16[32,8,8,128]{3,1,0,2:T(8,128)(2,1)} %copy.30), calls=%async_computation.1 | async-start | bytes 1048576 | tf_op jit(solution)/shard_map/all_to_all | solution.py:99
  84.4 13.4 %all-to-all-done.1 = bf16[32,8,8,128]{3,1,0,2:T(8,128)(2,1)S(1)} async-done(((bf16[32,8,8,128]{3,1,0,2:T(8,128)(2,1)}), bf16[32,8,8,128]{3,1,0,2:T(8,128)(2,1)S(1)}, u32[]{:S(2)}, u32[]{:S(2)}) %all-to-all-start.1) | async-done | bytes 524320 | tf_op jit(solution)/shard_map/all_to_all | solution.py:99
  97.8 3.6 %all-to-all-start.3 = ((bf16[32,8,8,128]{3,1,0,2:T(8,128)(2,1)}), bf16[32,8,8,128]{3,1,0,2:T(8,128)(2,1)S(1)}, u32[]{:S(2)}, u32[]{:S(2)}) async-start(bf16[32,8,8,128]{3,1,0,2:T(8,128)(2,1)} %copy.34), calls=%async_computation.3 | async-start | bytes 1048576 | tf_op jit(solution)/shard_map/all_to_all | solution.py:106
  103.0 13.1 %all-to-all-done.3 = bf16[32,8,8,128]{3,1,0,2:T(8,128)(2,1)S(1)} async-done(((bf16[32,8,8,128]{3,1,0,2:T(8,128)(2,1)}), bf16[32,8,8,128]{3,1,0,2:T(8,128)(2,1)S(1)}, u32[]{:S(2)}, u32[]{:S(2)}) %all-to-all-start.3) | async-done | bytes 524320 | tf_op jit(solution)/shard_map/all_to_all | solution.py:106
  116.1 3.5 %all-to-all-start.2 = ((bf16[256,4,256]{2,0,1:T(8,128)(2,1)}), bf16[256,4,256]{2,0,1:T(8,128)(2,1)S(1)}, u32[]{:S(2)}, u32[]{:S(2)}) async-start(bf16[256,4,256]{2,0,1:T(8,128)(2,1)} %copy.32), calls=%async_computation.2 | async-start | bytes 1048576 | tf_op jit(solution)/shard_map/all_to_all | solution.py:123
  121.2 7.2 %all-to-all-done.2 = bf16[256,4,256]{2,0,1:T(8,128)(2,1)S(1)} async-done(((bf16[256,4,256]{2,0,1:T(8,128)(2,1)}), bf16[256,4,256]{2,0,1:T(8,128)(2,1)S(1)}, u32[]{:S(2)}, u32[]{:S(2)}) %all-to-all-start.2) | async-done | bytes 524320 | tf_op jit(solution)/shard_map/all_to_all | solution.py:123
  128.4 3.5 %all-to-all-start.4 = ((bf16[256,4,256]{2,0,1:T(8,128)(2,1)}), bf16[256,4,256]{2,0,1:T(8,128)(2,1)S(1)}, u32[]{:S(2)}, u32[]{:S(2)}) async-start(bf16[256,4,256]{2,0,1:T(8,128)(2,1)} %copy.36), calls=%async_computation.4 | async-start | bytes 1048576 | tf_op jit(solution)/shard_map/all_to_all | solution.py:130
  131.9 1.4 fusion.44
  133.3 7.4 %all-to-all-done.4 = bf16[256,4,256]{2,0,1:T(8,128)(2,1)S(1)} async-done(((bf16[256,4,256]{2,0,1:T(8,128)(2,1)}), bf16[256,4,256]{2,0,1:T(8,128)(2,1)S(1)}, u32[]{:S(2)}, u32[]{:S(2)}) %all-to-all-start.4) | async-done | bytes 524320 | tf_op jit(solution)/shard_map/all_to_all | solution.py:130
  140.7 1.4 fusion.28
  142.1 1.0 reduce.1
  143.2 11.2 %all_to_all.81 = bf16[4,2,32768]{2,1,0:T(2,128)(2,1)S(1)} all-to-all(bf16[4,2,32768]{2,1,0:T(2,128)(2,1)S(1)} %reshape.106), channel_id=1, replica_groups=mesh['row'=8,'col'=4] {'col'}, dimensions={0} | all-to-all | bytes 1048576 | tf_op jit(solution)/shard_map/all_to_all | solution.py:149
  156.1 21.1 %all-gather.2.cloned.1.call-done = bf16[1024,1024]{0,1:T(8,128)(2,1)} async-done(((bf16[256,1024]{0,1:T(8,128)(2,1)}), bf16[1024,1024]{0,1:T(8,128)(2,1)}) %all-gather.2.cloned.1.call-update) | async-done | bytes 2097168 | tf_op jit(solution)/shard_map/all_gather | solution.py:151
  177.2 3.8 %convolution_convert_fusion = bf16[1024,512]{1,0:T(8,128)(2,1)} fusion(bf16[1024,1024]{0,1:T(8,128)(2,1)} %all-gather.2.cloned.1.call-done, bf16[1024,512]{1,0:T(8,128)(2,1)S(1)} %copy-done), kind=kOutput, calls=%fused_computation.35 | convolution fusion | flops 1074266112 | bytes 4194304 | tf_op jit(solution)/shard_map/dot_general | solution.py:150
  (35 shorter events, 11.6 us)
Async XLA Ops:
  6.5 170.6 %copy-start = (bf16[1024,512]{1,0:T(8,128)(2,1)S(1)}, bf16[1024,512]{1,0:T(8,128)(2,1)}, u32[]{:S(2)}) copy-start(bf16[1024,512]{1,0:T(8,128)(2,1)} %param.7) | copy-start | bytes 3145732
  6.5 3.5 %copy-start.1 = (bf16[1024,2048]{1,0:T(8,128)(2,1)S(1)}, bf16[1024,2048]{1,0:T(8,128)(2,1)}, u32[]{:S(2)}) copy-start(bf16[1024,2048]{1,0:T(8,128)(2,1)} %param.4) | copy-start | bytes 12582916
  6.5 3.5 %copy-start.2 = (f32[2048]{0:T(1024)S(1)}, f32[2048]{0:T(1024)}, u32[]{:S(2)}) copy-start(f32[2048]{0:T(1024)} %param.5) | copy-start | bytes 24580
  15.6 21.8 %all-to-all-start = ((bf16[8,2,16384]{2,1,0:T(2,128)(2,1)}), bf16[8,2,16384]{2,1,0:T(2,128)(2,1)S(1)}, u32[]{:S(2)}, u32[]{:S(2)}) async-start(bf16[8,2,16384]{2,1,0:T(2,128)(2,1)} %reshape.104), calls=%async_computation | async-start | bytes 1048576 | tf_op jit(solution)/shard_map/all_to_all | solution.py:80
  79.5 18.3 %all-to-all-start.1 = ((bf16[32,8,8,128]{3,1,0,2:T(8,128)(2,1)}), bf16[32,8,8,128]{3,1,0,2:T(8,128)(2,1)S(1)}, u32[]{:S(2)}, u32[]{:S(2)}) async-start(bf16[32,8,8,128]{3,1,0,2:T(8,128)(2,1)} %copy.30), calls=%async_computation.1 | async-start | bytes 1048576 | tf_op jit(solution)/shard_map/all_to_all | solution.py:99
  97.8 18.3 %all-to-all-start.3 = ((bf16[32,8,8,128]{3,1,0,2:T(8,128)(2,1)}), bf16[32,8,8,128]{3,1,0,2:T(8,128)(2,1)S(1)}, u32[]{:S(2)}, u32[]{:S(2)}) async-start(bf16[32,8,8,128]{3,1,0,2:T(8,128)(2,1)} %copy.34), calls=%async_computation.3 | async-start | bytes 1048576 | tf_op jit(solution)/shard_map/all_to_all | solution.py:106
  116.1 12.3 %all-to-all-start.2 = ((bf16[256,4,256]{2,0,1:T(8,128)(2,1)}), bf16[256,4,256]{2,0,1:T(8,128)(2,1)S(1)}, u32[]{:S(2)}, u32[]{:S(2)}) async-start(bf16[256,4,256]{2,0,1:T(8,128)(2,1)} %copy.32), calls=%async_computation.2 | async-start | bytes 1048576 | tf_op jit(solution)/shard_map/all_to_all | solution.py:123
  128.4 12.3 %all-to-all-start.4 = ((bf16[256,4,256]{2,0,1:T(8,128)(2,1)}), bf16[256,4,256]{2,0,1:T(8,128)(2,1)S(1)}, u32[]{:S(2)}, u32[]{:S(2)}) async-start(bf16[256,4,256]{2,0,1:T(8,128)(2,1)} %copy.36), calls=%async_computation.4 | async-start | bytes 1048576 | tf_op jit(solution)/shard_map/all_to_all | solution.py:130
  131.9 45.3 %all-gather.2.cloned.1.call-start = ((), (), s32[]{:S(2)}) async-start(), calls=%async_computation.6 | async-start | bytes 2621440 | tf_op jit(solution)/shard_map/all_gather | solution.py:151
Sparse Core Ops, SparseCore 0:
  156.2 20.9 all-gather.1
where the time goes:
time: 192 us; the launch traced here: 188 us
  waiting for transfers between devices  76.6 us (40%)
  matrix products  48.5 us (25%)
  starting transfers between devices  21.5 us (11%)
  between operations  13.8 us (7%)
  blocking collectives  11.2 us (6%)
  local copies, waits for them, and re-layouts  10.6 us (6%)
  other arithmetic  5.85 us (3%)
    all_gather x1, waiting for transfers between devices, local(): lax.all_gather(spectral.reshape(channels, length_dev), 'col', axis=0, til...  21.1 us
    dot_general x2, matrix products, second_section(): with_sin = jnp.dot(stacked, sine, precision=lax.Precision.HIGH)  19 us
    dot_general x2, matrix products, second_section(): with_cos = jnp.dot(stacked, cosine, precision=lax.Precision.HIGH)  18.9 us
    all_to_all x1, waiting for transfers between devices, local(): lax.all_to_all(projected.reshape(channels, 1, length_dev), 'row', split_a...  14.3 us
    all_to_all x1, waiting for transfers between devices, local(): lax.all_to_all(real_three.reshape(shaped).astype(jnp.bfloat16), 'row', sp...  13.4 us
    all_to_all x1, waiting for transfers between devices, local(): lax.all_to_all(imag_three.reshape(shaped).astype(jnp.bfloat16), 'row', sp...  13.1 us
    all_to_all x1, blocking collectives, local(): lax.all_to_all(result, 'col', split_axis=0, concat_axis=1, tiled=True)  11.2 us
    all_to_all x1, waiting for transfers between devices, local(): lax.all_to_all(as_sent(spec_imag.reshape(channels, col_count, quarter)),...  7.36 us
  transfers between devices with their start and end apart: 6, of which 6 were waited for; matrix products, arithmetic and copies ran while one was open for 3% of the time, Pallas kernels for 0%

commit v1 on v0

--- a/solution.py
+++ b/solution.py
@@ -1,8 +1,12 @@
+import functools
 import math
 
 import jax
 import jax.numpy as jnp
+import numpy as np
 from jax import lax
+from jax.experimental import pallas as pl
+from jax.experimental.pallas import tpu as pltpu
 from jax.sharding import PartitionSpec as P
 
 GROUP = 256
@@ -156,8 +160,320 @@
     return output.astype(jnp.bfloat16)
 
 
+HALVES = 2
+POINTS = 8
+LANES = 128
+MESH = pl.DeviceIdType.MESH
+
+
+def channel_tables(group, total_len):
+    half = group // 2
+    index = np.arange(group)
+    angle = 2.0 * np.pi * (index[:, None] * index[None, :] % group) / group
+    transform = np.concatenate([np.cos(angle[: half + 1]), np.sin(angle[1:half])], 0)
+    fold = np.zeros((group, group))
+    for k in range(half + 1):
+        fold[k, k] = 1.0
+        fold[k, -k % group] = 1.0
+    for k in range(1, half):
+        fold[half + k, group - k] = 1.0
+        fold[half + k, k] = -1.0
+    return (transform / math.sqrt(group)).astype(jnp.bfloat16), fold.astype(jnp.bfloat16)
+
+
+def position_tables(block, total_len):
+    j = np.arange(block)
+    angle = 2.0 * np.pi * (np.arange(POINTS)[:, None] * j[None, :]) / total_len
+    twiddles = np.stack([np.cos(angle), np.sin(angle)]).astype(np.float32)
+    root = 32
+    coarse = 2.0 * np.pi * (np.arange(block // root)[:, None] * root * j[None, :] % block) / block
+    fine = 2.0 * np.pi * (np.arange(root)[:, None] * j[None, :] % block) / block
+    scale = 1.0 / math.sqrt(total_len)
+    coarse = np.stack([np.cos(coarse), np.sin(coarse)]).astype(np.float32)
+    fine = np.stack([np.cos(fine) * scale, np.sin(fine) * scale]).astype(np.float32)
+    return twiddles, coarse, fine
+
+
+def eight_points(x):
+    a = [x[i] + x[i + 4] for i in range(4)]
+    b = [x[i] - x[i + 4] for i in range(4)]
+    even, odd = a[0] + a[2], a[1] + a[3]
+    root = math.sqrt(0.5)
+    minus, plus = root * (b[1] - b[3]), root * (b[1] + b[3])
+    one = (b[0] + minus, -b[2] - plus)
+    two = (a[0] - a[2], a[3] - a[1])
+    three = (b[0] - minus, b[2] - plus)
+    return [
+        (even + odd, None),
+        one,
+        two,
+        three,
+        (even - odd, None),
+        (three[0], -three[1]),
+        (two[0], -two[1]),
+        (one[0], -one[1]),
+    ]
+
+
+def mixer_kernel(
+    steps,
+    tokens_hbm, gain_hbm, w_in_hbm, w_out_hbm, forward_hbm, fold_hbm, twiddle_hbm, coarse_hbm, fine_hbm,
+    out_ref,
+    tokens, gain, w_in, w_out, forward, fold, twiddles, coarse, fine,
+    packed, arrived, stage, table, ready, gathered, folded, total,
+    token_sem, load_sem, own_sem, send_one, recv_one, send_two, recv_two, send_col, recv_col,
+):
+    row, col = lax.axis_index("row"), lax.axis_index("col")
+    rows = packed.shape[1]
+    block, width = packed.shape[3], w_in.shape[1]
+    size = block // steps
+    part = packed.shape[2]
+    flip = lambda bit: col + bit - 2 * bit * (col // bit % 2)
+    sibling, across = flip(1), flip(2)
+
+    loads = [
+        pltpu.make_async_copy(src, dst, load_sem.at[i])
+        for i, (src, dst) in enumerate([
+            (w_in_hbm, w_in), (gain_hbm, gain), (forward_hbm, forward), (coarse_hbm, coarse), (fine_hbm, fine),
+            (twiddle_hbm, twiddles), (fold_hbm, fold), (w_out_hbm, w_out),
+        ])
+    ]
+    token_loads = [
+        pltpu.make_async_copy(
+            tokens_hbm.at[pl.ds(p * size, size)], tokens.at[pl.ds(p * size, size)], token_sem.at[p]
+        )
+        for p in range(steps)
+    ]
+    for load in loads[:3]:
+        load.start()
+    for load in token_loads:
+        load.start()
+    for load in loads[3:]:
+        load.start()
+
+    barrier = pltpu.get_barrier_semaphore()
+    peers = [(lax.rem(row + d, rows), col) for d in range(1, rows)] + [(row, sibling), (row, across)]
+    for peer in peers:
+        pl.semaphore_signal(barrier, inc=1, device_id=peer, device_id_type=MESH)
+
+    def remote(src, dst, send, recv, device):
+        return pltpu.make_async_remote_copy(
+            src_ref=src, dst_ref=dst, send_sem=send, recv_sem=recv, device_id=device, device_id_type=MESH
+        )
+
+    def first_send(h, d, p=None):
+        peer = lax.rem(row + d, rows)
+        where = pl.ds(0, block) if p is None else pl.ds(p * size, size)
+        return remote(
+            packed.at[h, peer, :, where], arrived.at[h, row, :, where],
+            send_one.at[h, d], recv_one.at[h, d], (peer, col),
+        )
+
+    order = [4, 3, 5, 2, 6, 1, 7]
+    for load in loads[:3]:
+        load.wait()
+    for p in range(steps):
+        token_loads[p].wait()
+        where = slice(p * size, (p + 1) * size)
+        wide = tokens[where, :].astype(jnp.float32)
+        inverse = lax.rsqrt(jnp.mean(wide * wide, axis=1, keepdims=True) + NORM_EPS)
+        normed = (wide * inverse * gain[...]).astype(jnp.bfloat16)
+        projected = jnp.dot(normed, w_in[...], preferred_element_type=jnp.float32).astype(jnp.bfloat16)
+        kept = lax.dot_general(
+            forward[...], projected, (((1,), (1,)), ((), ())), preferred_element_type=jnp.float32
+        )
+        packed[:, :, :, where] = kept.astype(jnp.bfloat16).reshape(HALVES, rows, part, size)
+        if p == 0:
+            pl.semaphore_wait(barrier, len(peers))
+        for d in order:
+            first_send(0, d, p).start()
+    for d in order:
+        first_send(1, d).start()
+    own_one = [
+        pltpu.make_async_copy(packed.at[h, row], arrived.at[h, row], own_sem.at[h]) for h in range(HALVES)
+    ]
+    for copy in own_one:
+        copy.start()
+    for load in loads[3:]:
+        load.wait()
+
+    root = fine.shape[1]
+
+    def table_rows(a, carry):
+        cos_a, sin_a = coarse[0, pl.ds(a, 1), :], coarse[1, pl.ds(a, 1), :]
+        at = pl.multiple_of(a * root, root)
+        table[pl.ds(at, root), :] = (cos_a * fine[0] - sin_a * fine[1]).astype(jnp.bfloat16)
+        table[pl.ds(block + at, root), :] = (sin_a * fine[0] + cos_a * fine[1]).astype(jnp.bfloat16)
+        return carry
+
+    lax.fori_loop(0, block // root, table_rows, 0)
+    cols = w_out.shape[0] // width
+    half = width // HALVES
+    for c in range(cols):
+        rows_out = jnp.dot(
+            fold[...], w_out[c * width : (c + 1) * width, :], preferred_element_type=jnp.float32
+        ).astype(jnp.bfloat16)
+        for h in range(HALVES):
+            folded[h, c * half : (c + 1) * half, :] = rows_out[h * half : (h + 1) * half]
+
+    def second_send(h, d):
+        peer = lax.rem(row + d, rows)
+        return remote(
+            ready.at[h, peer], gathered.at[h, col, row], send_two.at[h, d], recv_two.at[h, d], (peer, col)
+        )
+
+    own_two = [
+        pltpu.make_async_copy(ready.at[h, row], gathered.at[h, col, row], own_sem.at[HALVES + h])
+        for h in range(HALVES)
+    ]
+    for h in range(HALVES):
+        own_one[h].wait()
+        for d in order:
+            first_send(h, d).wait_recv()
+
+        def section(t, carry):
+            at = pl.multiple_of(t * LANES, LANES)
+            x = [arrived[h, r, :, pl.ds(at, LANES)].astype(jnp.float32) for r in range(rows)]
+            points = eight_points(x)
+            for k in range(POINTS):
+                real, imag = points[k]
+                if k > 0:
+                    cosine = twiddles[0, k : k + 1, pl.ds(at, LANES)]
+                    sine = twiddles[1, k : k + 1, pl.ds(at, LANES)]
+                    if imag is None:
+                        real, imag = real * cosine, -real * sine
+                    else:
+                        real, imag = real * cosine + imag * sine, imag * cosine - real * sine
+                else:
+                    imag = jnp.zeros_like(real)
+                if h == 1:
+                    place = lax.broadcasted_iota(jnp.int32, real.shape, 0) + row * part
+                    plain = place == 0
+                    real, imag = jnp.where(plain, real, -imag), jnp.where(plain, imag, real)
+                stage[k, :, pl.ds(at, LANES)] = real.astype(jnp.bfloat16)
+                stage[k, :, pl.ds(pl.multiple_of(block + at, LANES), LANES)] = imag.astype(jnp.bfloat16)
+            return carry
+
+        lax.fori_loop(0, block // LANES, section, 0)
+        values = stage[...].reshape(POINTS * part, 2 * block)
+        span = 2 * LANES
+        for n in range(block // span):
+            done = jnp.dot(
+                values, table[:, n * span : (n + 1) * span], preferred_element_type=jnp.float32
+            ).astype(jnp.bfloat16)
+            for q in range(2):
+                ready[h, 2 * n + q] = done[:, q * LANES : (q + 1) * LANES].reshape(POINTS, part, LANES)
+        for d in order:
+            second_send(h, d).start()
+        own_two[h].start()
+
+    def to_across(h, d, origin):
+        spot = gathered.at[h, col, origin]
+        return remote(spot, spot, send_col.at[h, 0, d], recv_col.at[h, 0, d], (row, across))
+
+    def to_sibling(h, d, origin):
+        spot = gathered.at[h, col, origin]
+        return remote(spot, spot, send_col.at[h, 1, d], recv_col.at[h, 1, d], (row, sibling))
+
+    def on_to_sibling(h, d, origin):
+        spot = gathered.at[h, across, origin]
+        return remote(spot, spot, send_col.at[h, 2, d], recv_col.at[h, 2, d], (row, sibling))
+
+    near = [0, 1, 7, 2, 6, 3, 5, 4]
+    origin_of = lambda d: lax.rem(row + rows - d, rows)
+    for h in range(HALVES):
+        for d in near:
+            if d == 0:
+                own_two[h].wait()
+            else:
+                second_send(h, d).wait_recv()
+            to_across(h, d, origin_of(d)).start()
+            to_sibling(h, d, origin_of(d)).start()
+        for d in near:
+            to_across(h, d, origin_of(d)).wait_recv()
+            on_to_sibling(h, d, origin_of(d)).start()
+        for d in near:
+            to_sibling(h, d, origin_of(d)).wait_recv()
+            on_to_sibling(h, d, origin_of(d)).wait_recv()
+        for k in range(POINTS):
+            spectrum = gathered[h, :, :, k].reshape(cols * rows * part, LANES)
+            piece = lax.dot_general(
+                spectrum, folded[h], (((0,), (0,)), ((), ())), preferred_element_type=jnp.float32
+            )
+            if h == 0:
+                total[k] = piece
+            else:
+                scattered = total[k] + piece
+                total[k] = scattered
+    out_ref[...] = jnp.swapaxes(total[...], 0, 1).reshape(out_ref.shape).astype(out_ref.dtype)
+
+    for h in range(HALVES):
+        for d in order:
+            first_send(h, d).wait_send()
+            second_send(h, d).wait_send()
+        for d in near:
+            to_across(h, d, origin_of(d)).wait_send()
+            to_sibling(h, d, origin_of(d)).wait_send()
+            on_to_sibling(h, d, origin_of(d)).wait_send()
+
+
+def fused(tokens, norm_gain, w_in, w_out):
+    rows, cols = lax.axis_size("row"), lax.axis_size("col")
+    block, width_in = tokens.shape
+    width = w_in.shape[1]
+    features = w_out.shape[1]
+    part = width // (HALVES * rows)
+    steps = 4
+    forward, fold = channel_tables(width, block * rows)
+    twiddles, coarse, fine = position_tables(block, block * rows)
+    half, short, wide = jnp.bfloat16, pltpu.VMEM, jnp.float32
+    operands = [tokens, norm_gain[None, :], w_in, w_out, forward, fold, twiddles, coarse, fine]
+    operands = [jnp.asarray(x) for x in operands]
+    dma = pltpu.SemaphoreType.DMA
+    return pl.pallas_call(
+        functools.partial(mixer_kernel, steps),
+        out_shape=jax.ShapeDtypeStruct((block, features), half),
+        in_specs=[pl.BlockSpec(memory_space=pl.ANY)] * len(operands),
+        out_specs=pl.BlockSpec(memory_space=pltpu.VMEM),
+        scratch_shapes=[short(x.shape, x.dtype) for x in operands]
+        + [
+            short((HALVES, rows, part, block), half),
+            short((HALVES, rows, part, block), half),
+            short((POINTS, part, 2 * block), half),
+            short((2 * block, block), half),
+            short((HALVES, rows, POINTS, part, LANES), half),
+            short((HALVES, cols, rows, POINTS, part, LANES), half),
+            short((HALVES, w_out.shape[0] // HALVES, features), half),
+            short((POINTS, LANES, features), wide),
+            dma((steps,)),
+            dma((8,)),
+            dma((2 * HALVES,)),
+            dma((HALVES, rows)),
+            dma((HALVES, rows)),
+            dma((HALVES, rows)),
+            dma((HALVES, rows)),
+            dma((HALVES, 3, rows)),
+            dma((HALVES, 3, rows)),
+        ],
+        compiler_params=pltpu.CompilerParams(
+            collective_id=0, has_side_effects=True, vmem_limit_bytes=60 * 1024 * 1024
+        ),
+    )(*operands)
+
+
+def fits(mesh):
+    return mesh.shape["row"] == POINTS and mesh.shape["col"] == 4
+
+
+def choose(mesh, *arrays):
+    tokens, _, w_in, _ = arrays
+    group_local = w_in.shape[1] == GROUP
+    tiles = tokens.shape[0] == POINTS * LANES
+    return fused(*arrays) if fits(mesh) and group_local and tiles else local(*arrays)
+
+
 def solution(mesh):
     placed = (P("row", None), P(), P(None, "col"), P(None, "col"))
     return jax.shard_map(
-        local, mesh=mesh, in_specs=placed, out_specs=P("row", "col"), check_vma=False
-    )
+        functools.partial(choose, mesh), mesh=mesh, in_specs=placed, out_specs=P("row", "col"), check_vma=False
+    )

time: 192 us -> 46.9 us (0.24)
  the two profiles are of different devices: /device:TPU:0 before, /device:TPU:11 now
where the time goes in v1:
time: 46.9 us; the launch traced here: 46.8 us
  Pallas kernels  44.5 us (95%)
  local copies, waits for them, and re-layouts  2.26 us (5%)
    pallas_call x1, Pallas kernels, fused(): pl.pallas_call(functools.partial(mixer_kernel, steps), out_shape=jax.Shap...  44.5 us
    unnamed x1, local copies, waits for them, and re-layouts  2.26 us

profile of v1, /device:TPU:11, one launch (start us, length us, event | category | flops | bytes accessed | tf_op | source)
XLA Modules:
  0.0 46.8 jit_solution(9386660265261745231)
XLA Ops:
  0.0 44.5 %shard_map.91 = bf16[1024,512]{1,0:T(8,128)(2,1)} custom-call(bf16[1024,2048]{1,0:T(8,128)(2,1)} %tokens_hbm.1, f32[1,2048]{1,0:T(1,128)} %bitcast.1, bf16[2048,256]{1,0:T(8,128)(2,1)} %w_in_hbm.1, bf16[1024,512]{1,0:T(8,128)(2,1)} %w_out_hbm.1, bf16[256,256]{1,0:T(8,128)(2,1)} %constant.10.clone.forward_hbm, bf16[256,256]{1,0:T(8,128)(2,1)} %constant.11.clone.fold_hbm, ...), custom_call_target="tpu_custom_call" | custom-call | tf_op jit(solution)/shard_map/pallas_call | solution.py:433
  44.5 2.3 %copy.11 = bf16[1024,512]{1,0:T(8,128)(2,1)} copy(bf16[1024,512]{1,0:T(8,128)(2,1)} %shard_map.91) | data formatting | bytes 2097152

commit v2 on v1

--- a/solution.py
+++ b/solution.py
@@ -162,6 +162,7 @@
 
 HALVES = 2
 POINTS = 8
+SPLIT = 1
 LANES = 128
 MESH = pl.DeviceIdType.MESH
 
@@ -216,7 +217,7 @@
 
 
 def mixer_kernel(
-    steps,
+    steps, ahead,
     tokens_hbm, gain_hbm, w_in_hbm, w_out_hbm, forward_hbm, fold_hbm, twiddle_hbm, coarse_hbm, fine_hbm,
     out_ref,
     tokens, gain, w_in, w_out, forward, fold, twiddles, coarse, fine,
@@ -228,8 +229,15 @@
     block, width = packed.shape[3], w_in.shape[1]
     size = block // steps
     part = packed.shape[2]
-    flip = lambda bit: col + bit - 2 * bit * (col // bit % 2)
-    sibling, across = flip(1), flip(2)
+    flip = lambda index, bit: index + bit - 2 * bit * (index // bit % 2)
+    sibling, across = flip(col, 1), flip(col, 2)
+
+    def mate(d):
+        index = row
+        for bit in (1, 2, 4):
+            if d & bit:
+                index = flip(index, bit)
+        return index
 
     loads = [
         pltpu.make_async_copy(src, dst, load_sem.at[i])
@@ -244,15 +252,11 @@
         )
         for p in range(steps)
     ]
-    for load in loads[:3]:
+    for load in loads[:3] + token_loads[:ahead]:
         load.start()
-    for load in token_loads:
-        load.start()
-    for load in loads[3:]:
-        load.start()
 
     barrier = pltpu.get_barrier_semaphore()
-    peers = [(lax.rem(row + d, rows), col) for d in range(1, rows)] + [(row, sibling), (row, across)]
+    peers = [(mate(d), col) for d in range(1, rows)] + [(row, sibling), (row, across)]
     for peer in peers:
         pl.semaphore_signal(barrier, inc=1, device_id=peer, device_id_type=MESH)
 
@@ -262,18 +266,23 @@
         )
 
     def first_send(h, d, p=None):
-        peer = lax.rem(row + d, rows)
+        peer = mate(d)
         where = pl.ds(0, block) if p is None else pl.ds(p * size, size)
         return remote(
             packed.at[h, peer, :, where], arrived.at[h, row, :, where],
             send_one.at[h, d], recv_one.at[h, d], (peer, col),
         )
 
-    order = [4, 3, 5, 2, 6, 1, 7]
+    order = [4, 5, 6, 7, 2, 3, 1]
     for load in loads[:3]:
         load.wait()
     for p in range(steps):
         token_loads[p].wait()
+        if p + ahead < steps:
+            token_loads[p + ahead].start()
+        elif p + ahead == steps:
+            for load in loads[3:]:
+                load.start()
         where = slice(p * size, (p + 1) * size)
         wide = tokens[where, :].astype(jnp.float32)
         inverse = lax.rsqrt(jnp.mean(wide * wide, axis=1, keepdims=True) + NORM_EPS)
@@ -316,16 +325,26 @@
         for h in range(HALVES):
             folded[h, c * half : (c + 1) * half, :] = rows_out[h * half : (h + 1) * half]
 
-    def second_send(h, d):
-        peer = lax.rem(row + d, rows)
+    cut = POINTS // SPLIT
+
+    def second_send(g, d):
+        h, where = g // SPLIT, pl.ds(g % SPLIT * cut, cut)
+        peer = mate(d)
         return remote(
-            ready.at[h, peer], gathered.at[h, col, row], send_two.at[h, d], recv_two.at[h, d], (peer, col)
-        )
-
-    own_two = [
-        pltpu.make_async_copy(ready.at[h, row], gathered.at[h, col, row], own_sem.at[HALVES + h])
-        for h in range(HALVES)
-    ]
+            ready.at[h, peer, where], gathered.at[h, col, row, where],
+            send_two.at[g, d], recv_two.at[g, d], (peer, col),
+        )
+
+    def keep(g):
+        h, where = g // SPLIT, pl.ds(g % SPLIT * cut, cut)
+        return pltpu.make_async_copy(
+            ready.at[h, row, where], gathered.at[h, col, row, where], own_sem.at[HALVES + g]
+        )
+
+    span = 2 * LANES
+    count = block // span
+    other = (1 - row // (rows // 2)) * (count // 2)
+    far, close = order[: rows // 2], order[rows // 2 :]
     for h in range(HALVES):
         own_one[h].wait()
         for d in order:
@@ -356,65 +375,89 @@
 
         lax.fori_loop(0, block // LANES, section, 0)
         values = stage[...].reshape(POINTS * part, 2 * block)
-        span = 2 * LANES
-        for n in range(block // span):
+        for i in range(count):
+            n = lax.rem(other + i, count)
             done = jnp.dot(
-                values, table[:, n * span : (n + 1) * span], preferred_element_type=jnp.float32
+                values, table[:, pl.ds(pl.multiple_of(n * span, span), span)], preferred_element_type=jnp.float32
             ).astype(jnp.bfloat16)
             for q in range(2):
                 ready[h, 2 * n + q] = done[:, q * LANES : (q + 1) * LANES].reshape(POINTS, part, LANES)
-        for d in order:
-            second_send(h, d).start()
-        own_two[h].start()
-
-    def to_across(h, d, origin):
-        spot = gathered.at[h, col, origin]
-        return remote(spot, spot, send_col.at[h, 0, d], recv_col.at[h, 0, d], (row, across))
-
-    def to_sibling(h, d, origin):
-        spot = gathered.at[h, col, origin]
-        return remote(spot, spot, send_col.at[h, 1, d], recv_col.at[h, 1, d], (row, sibling))
-
-    def on_to_sibling(h, d, origin):
-        spot = gathered.at[h, across, origin]
-        return remote(spot, spot, send_col.at[h, 2, d], recv_col.at[h, 2, d], (row, sibling))
-
-    near = [0, 1, 7, 2, 6, 3, 5, 4]
-    origin_of = lambda d: lax.rem(row + rows - d, rows)
-    for h in range(HALVES):
-        for d in near:
+            if i == count // 2 - 1:
+                for g in range(h * SPLIT, (h + 1) * SPLIT):
+                    for d in far:
+                        second_send(g, d).start()
+        for g in range(h * SPLIT, (h + 1) * SPLIT):
+            for d in close:
+                second_send(g, d).start()
+            keep(g).start()
+
+    def along(g, way, owner, target, d):
+        spot = gathered.at[g // SPLIT, owner, mate(d), pl.ds(g % SPLIT * cut, cut)]
+        return remote(spot, spot, send_col.at[g, way, d], recv_col.at[g, way, d], (row, target))
+
+    def to_across(g, d):
+        return along(g, 0, col, across, d)
+
+    def to_sibling(g, d):
+        return along(g, 1, col, sibling, d)
+
+    def on_to_sibling(g, d):
+        return along(g, 2, across, sibling, d)
+
+    near, every = [0] + close[::-1], [0] + close[::-1] + far
+
+    def relay(g, origins):
+        for d in origins:
             if d == 0:
-                own_two[h].wait()
+                keep(g).wait()
             else:
-                second_send(h, d).wait_recv()
-            to_across(h, d, origin_of(d)).start()
-            to_sibling(h, d, origin_of(d)).start()
-        for d in near:
-            to_across(h, d, origin_of(d)).wait_recv()
-            on_to_sibling(h, d, origin_of(d)).start()
-        for d in near:
-            to_sibling(h, d, origin_of(d)).wait_recv()
-            on_to_sibling(h, d, origin_of(d)).wait_recv()
-        for k in range(POINTS):
-            spectrum = gathered[h, :, :, k].reshape(cols * rows * part, LANES)
-            piece = lax.dot_general(
-                spectrum, folded[h], (((0,), (0,)), ((), ())), preferred_element_type=jnp.float32
-            )
-            if h == 0:
-                total[k] = piece
-            else:
-                scattered = total[k] + piece
-                total[k] = scattered
+                second_send(g, d).wait_recv()
+            to_across(g, d).start()
+            to_sibling(g, d).start()
+
+    def pass_on(g, origins):
+        for d in origins:
+            to_across(g, d).wait_recv()
+            on_to_sibling(g, d).start()
+
+    def collect(g):
+        for d in every:
+            to_sibling(g, d).wait_recv()
+            on_to_sibling(g, d).wait_recv()
+
+    def map_out(h, k):
+        spectrum = gathered[h, :, :, k].reshape(cols * rows * part, LANES)
+        piece = lax.dot_general(
+            spectrum, folded[h], (((0,), (0,)), ((), ())), preferred_element_type=jnp.float32
+        )
+        total[k] = piece if h == 0 else total[k] + piece
+
+    def map_part(g):
+        for k in range(g % SPLIT * cut, (g % SPLIT + 1) * cut):
+            map_out(g // SPLIT, k)
+
+    relay(0, every)
+    for d in every:
+        relay(1, [d])
+        pass_on(0, [d])
+    collect(0)
+    for k, d in enumerate(every):
+        map_out(0, k)
+        pass_on(1, [d])
+    collect(1)
+    map_part(1)
     out_ref[...] = jnp.swapaxes(total[...], 0, 1).reshape(out_ref.shape).astype(out_ref.dtype)
 
     for h in range(HALVES):
         for d in order:
             first_send(h, d).wait_send()
-            second_send(h, d).wait_send()
-        for d in near:
-            to_across(h, d, origin_of(d)).wait_send()
-            to_sibling(h, d, origin_of(d)).wait_send()
-            on_to_sibling(h, d, origin_of(d)).wait_send()
+    for g in range(HALVES * SPLIT):
+        for d in order:
+            second_send(g, d).wait_send()
+        for d in every:
+            to_across(g, d).wait_send()
+            to_sibling(g, d).wait_send()
+            on_to_sibling(g, d).wait_send()
 
 
 def fused(tokens, norm_gain, w_in, w_out):
@@ -431,7 +474,7 @@
     operands = [jnp.asarray(x) for x in operands]
     dma = pltpu.SemaphoreType.DMA
     return pl.pallas_call(
-        functools.partial(mixer_kernel, steps),
+        functools.partial(mixer_kernel, steps, 2),
         out_shape=jax.ShapeDtypeStruct((block, features), half),
         in_specs=[pl.BlockSpec(memory_space=pl.ANY)] * len(operands),
         out_specs=pl.BlockSpec(memory_space=pltpu.VMEM),
@@ -447,13 +490,13 @@
             short((POINTS, LANES, features), wide),
             dma((steps,)),
             dma((8,)),
-            dma((2 * HALVES,)),
+            dma((HALVES + HALVES * SPLIT,)),
             dma((HALVES, rows)),
             dma((HALVES, rows)),
-            dma((HALVES, rows)),
-            dma((HALVES, rows)),
-            dma((HALVES, 3, rows)),
-            dma((HALVES, 3, rows)),
+            dma((HALVES * SPLIT, rows)),
+            dma((HALVES * SPLIT, rows)),
+            dma((HALVES * SPLIT, 3, rows)),
+            dma((HALVES * SPLIT, 3, rows)),
         ],
         compiler_params=pltpu.CompilerParams(
             collective_id=0, has_side_effects=True, vmem_limit_bytes=60 * 1024 * 1024

time: 46.9 us -> 43 us (0.917)
  the two profiles are of different devices: /device:TPU:11 before, /device:TPU:0 now
where the time goes in v2:
time: 43 us; the launch traced here: 42.2 us
  Pallas kernels  39.9 us (93%)
  local copies, waits for them, and re-layouts  2.26 us (5%)
    pallas_call x1, Pallas kernels, fused(): pl.pallas_call(functools.partial(mixer_kernel, steps, 2), out_shape=jax.S...  39.9 us
    unnamed x1, local copies, waits for them, and re-layouts  2.26 us

profile of v2, /device:TPU:0, one launch (start us, length us, event | category | flops | bytes accessed | tf_op | source)
XLA Modules:
  0.0 42.2 jit_solution(4133393007618009898)
XLA Ops:
  0.0 39.9 %shard_map.91 = bf16[1024,512]{1,0:T(8,128)(2,1)} custom-call(bf16[1024,2048]{1,0:T(8,128)(2,1)} %tokens_hbm.1, f32[1,2048]{1,0:T(1,128)} %bitcast.1, bf16[2048,256]{1,0:T(8,128)(2,1)} %w_in_hbm.1, bf16[1024,512]{1,0:T(8,128)(2,1)} %w_out_hbm.1, bf16[256,256]{1,0:T(8,128)(2,1)} %constant.10.clone.forward_hbm, bf16[256,256]{1,0:T(8,128)(2,1)} %constant.11.clone.fold_hbm, ...), custom_call_target="tpu_custom_call" | custom-call | tf_op jit(solution)/shard_map/pallas_call | solution.py:476
  39.9 2.3 %copy.11 = bf16[1024,512]{1,0:T(8,128)(2,1)} copy(bf16[1024,512]{1,0:T(8,128)(2,1)} %shard_map.91) | data formatting | bytes 2097152
